TPU v7x, 32 devices: a whole 2x2x4 slice. The times are simulated.
32 devices in a mesh: sp: 4 (over y, x), tp: 8 (over z, core).
Axes of the slice: x: 2, y: 2, z: 4, core: 2. Of those that a mesh axis runs over, the one named last changes fastest.
Arguments:
- queries: bfloat16 [4096, 2048], P('sp', 'tp'), may hold values from -160 to 160
- key_heads: bfloat16 [4096, 512], P('sp'), may hold values from -8 to 8
- value_heads: bfloat16 [4096, 512], P('sp'), may hold values from -4 to 4
- sink_logit: float32 [16], P('tp'), may hold values from -2 to 7
- out_weight: bfloat16 [2048, 2048], P('tp'), may hold values from -0.125 to 0.125
- residual: bfloat16 [4096, 2048], P(('sp', 'tp')), may hold values from -6 to 6
- mixer_gain: float32 [2048], replicated, may hold values from 0.1 to 1.9
- expert_gain: float32 [2048], replicated, may hold values from 0.1 to 1.9
- route_group: int32 [4096], P(('sp', 'tp')), may hold values from 0 to 3, as said below
- route_member: int32 [4096, 2], P(('sp', 'tp')), may hold values from 0 to 2, as said below
- route_weight: bfloat16 [4096, 2], P(('sp', 'tp')), may hold values from 0.19921875 to 1
- gate_weight: bfloat16 [12, 2048, 2048], P('sp', None, 'tp'), may hold values from -0.125 to 0.125
- up_weight: bfloat16 [12, 2048, 2048], P('sp', None, 'tp'), may hold values from -0.125 to 0.125
- down_weight: bfloat16 [12, 2048, 2048], P('sp', 'tp'), may hold values from -0.125 to 0.125
Outputs:
- output: bfloat16 [4096, 2048], P(('sp', 'tp'))
Inputs may be any that keep to these rules, and one draw needn't show every extreme that they name: `route_group`: among the tokens of one device, at most 40 name one group; in every draw one group is named by exactly 40 tokens of every device. `route_member`: the two entries of a token are different members of its group.
All inputs are finite; a program needn't handle non-finite values.
Results may differ from a plain program's by a relative error of at most 0.018.
Values may be sent and summed in bfloat16 or wider, within the bound.
A program may use at most 128 MiB of HBM per device.

v0:
```python
import jax
import jax.numpy as jnp
from jax import lax
from jax.sharding import PartitionSpec as P

HEADS = 16
KV_HEADS = 4
HEAD_DIM = 128
WINDOW = 128
BLOCK = 128
GROUP_EXPERTS = 3


EPS = 1e-06
NEG_BIG = -1e30


def extended(block, sides, width):
    for axis, dim in sides:
        count = lax.axis_size(axis)
        forward = [(i, i + 1) for i in range(count - 1)]
        backward = [(target, source) for source, target in forward]
        low = lax.ppermute(
            lax.slice_in_dim(block, block.shape[dim] - width, None, axis=dim), axis, forward
        )
        high = lax.ppermute(lax.slice_in_dim(block, 0, width, axis=dim), axis, backward)
        block = jnp.concatenate([low, block, high], axis=dim)
    return block


def window_attention(queries, key_heads, value_heads, sink_logit):
    seq_rows = queries.shape[0]
    heads_dev = sink_logit.shape[0]
    key_group = HEADS // KV_HEADS
    key_start = lax.axis_index("tp") * heads_dev // key_group * HEAD_DIM
    key_own = lax.dynamic_slice_in_dim(key_heads, key_start, HEAD_DIM, 1)
    value_own = lax.dynamic_slice_in_dim(value_heads, key_start, HEAD_DIM, 1)
    padded = extended(jnp.stack([key_own, value_own]), (("sp", 1),), WINDOW)
    blocks = seq_rows // BLOCK
    extent = WINDOW // BLOCK
    tile_rows = padded.reshape(2, blocks + 2 * extent, BLOCK, HEAD_DIM)
    key_spans = jnp.concatenate(
        [tile_rows[:, shifted : shifted + blocks] for shifted in range(2 * extent + 1)], axis=2
    )
    offset = lax.axis_index("sp") * seq_rows
    seq_total = seq_rows * lax.axis_size("sp")
    query_pos = offset + jnp.arange(seq_rows, dtype=jnp.int32).reshape(blocks, BLOCK)
    key_pos = (
        offset
        + (jnp.arange(blocks, dtype=jnp.int32) * BLOCK)[:, None]
        + jnp.arange(BLOCK + 2 * WINDOW, dtype=jnp.int32)[None, :]
        - WINDOW
    )
    inside = (
        (jnp.abs(query_pos[:, :, None] - key_pos[:, None, :]) <= WINDOW)
        & (key_pos >= 0)[:, None, :]
        & (key_pos < seq_total)[:, None, :]
    )
    query_blocks = queries.reshape(blocks, BLOCK, heads_dev, HEAD_DIM)
    scores = jnp.einsum(
        "nqhd,nkd->nhqk", query_blocks, key_spans[0], preferred_element_type=jnp.float32
    ) * HEAD_DIM ** (-0.5)
    scores = jnp.where(inside[:, None], scores, NEG_BIG)
    sink_col = sink_logit[None, :, None, None]
    row_top = jnp.maximum(jnp.max(scores, axis=3, keepdims=True), sink_col)
    exp_terms = jnp.exp(scores - row_top)
    row_mass = jnp.sum(exp_terms, axis=3, keepdims=True) + jnp.exp(sink_col - row_top)
    weight = (exp_terms / row_mass).astype(jnp.bfloat16)
    attended = jnp.einsum(
        "nhqk,nkd->nqhd", weight, key_spans[1], preferred_element_type=jnp.float32
    ).astype(jnp.bfloat16)
    return attended.reshape(seq_rows, heads_dev * HEAD_DIM)


def per_device(
    queries,
    key_heads,
    value_heads,
    sink_logit,
    out_weight,
    residual,
    mixer_gain,
    expert_gain,
    route_group,
    route_member,
    route_weight,
    gate_weight,
    up_weight,
    down_weight,
):
    attended = window_attention(queries, key_heads, value_heads, sink_logit)
    tok_rows = residual.shape[0]
    width = out_weight.shape[1]
    projected = lax.psum_scatter(
        jnp.dot(attended, out_weight, preferred_element_type=jnp.float32).astype(jnp.bfloat16),
        "tp",
        scatter_dimension=0,
        tiled=True,
    ).astype(jnp.float32)
    proj_scale = lax.rsqrt(jnp.mean(projected * projected, axis=1, keepdims=True) + EPS)
    mixed_rows = (residual.astype(jnp.float32) + mixer_gain * (projected * proj_scale)).astype(
        jnp.bfloat16
    )
    mixed_float = mixed_rows.astype(jnp.float32)
    norm_scale = lax.rsqrt(jnp.mean(mixed_float * mixed_float, axis=1, keepdims=True) + EPS)
    normed = (mixed_float * norm_scale * expert_gain).astype(jnp.bfloat16)
    groups = lax.axis_size("sp")
    capacity = max(2, (5 * tok_rows + 4 * groups - 1) // (4 * groups))
    group_ids = jnp.arange(groups, dtype=jnp.int32)
    chosen = (route_group[:, None] == group_ids[None, :]).astype(jnp.int32)
    group_rank = jnp.sum(chosen * (jnp.cumsum(chosen, axis=0) - 1), axis=1)
    slot_ids = route_group * capacity + group_rank
    placing = (jnp.arange(groups * capacity, dtype=jnp.int32)[:, None] == slot_ids[None, :]).astype(
        jnp.bfloat16
    )
    member_ids = jnp.arange(GROUP_EXPERTS, dtype=jnp.int32)
    token_gates = jnp.sum(
        route_weight.astype(jnp.float32)[:, :, None]
        * (route_member[:, :, None] == member_ids[None, None, :]).astype(jnp.float32),
        axis=1,
    ).astype(jnp.bfloat16)
    send_rows = (
        jnp.dot(placing, normed, preferred_element_type=jnp.float32)
        .astype(jnp.bfloat16)
        .reshape(groups, capacity, width)
    )
    send_gates = (
        jnp.dot(placing, token_gates, preferred_element_type=jnp.float32)
        .astype(jnp.bfloat16)
        .reshape(groups, capacity, GROUP_EXPERTS)
    )
    arrived_rows, arrived_gates = (
        lax.all_to_all(send_rows, "sp", split_axis=0, concat_axis=0, tiled=True),
        lax.all_to_all(send_gates, "sp", split_axis=0, concat_axis=0, tiled=True),
    )
    pooled_rows, pooled_gates = (
        lax.all_gather(arrived_rows, "tp", axis=0, tiled=True),
        lax.all_gather(arrived_gates, "tp", axis=0, tiled=True),
    )
    flat_rows = pooled_rows.reshape(-1, width)
    flat_gates = pooled_gates.reshape(-1, GROUP_EXPERTS).astype(jnp.float32)
    gate_pre = jnp.einsum("md,edh->meh", flat_rows, gate_weight, preferred_element_type=jnp.float32)
    up_pre = jnp.einsum("md,edh->meh", flat_rows, up_weight, preferred_element_type=jnp.float32)
    hidden = (jax.nn.silu(gate_pre) * up_pre * flat_gates[:, :, None]).astype(jnp.bfloat16)
    partial_out = jnp.einsum("meh,ehd->md", hidden, down_weight, preferred_element_type=jnp.float32)
    summed = lax.psum_scatter(
        partial_out.reshape(pooled_rows.shape).astype(jnp.bfloat16),
        "tp",
        scatter_dimension=0,
        tiled=True,
    )
    returned = lax.all_to_all(summed, "sp", split_axis=0, concat_axis=0, tiled=True)
    expert_out = lax.dot_general(
        placing,
        returned.reshape(groups * capacity, width),
        (((0,), (0,)), ((), ())),
        preferred_element_type=jnp.float32,
    )
    return (mixed_float + expert_out).astype(jnp.bfloat16)


def solution(mesh):
    placed = (
        P("sp", "tp"),
        P("sp", None),
        P("sp", None),
        P("tp"),
        P("tp", None),
        P(("sp", "tp"), None),
        P(),
        P(),
        P(("sp", "tp")),
        P(("sp", "tp"), None),
        P(("sp", "tp"), None),
        P("sp", None, "tp"),
        P("sp", None, "tp"),
        P("sp", "tp", None),
    )
    return jax.shard_map(
        per_device, mesh=mesh, in_specs=placed, out_specs=P(("sp", "tp"), None), check_vma=False
    )
```

profile of v0, /device:TPU:16, one launch (start us, length us, event | category | flops | bytes accessed | tf_op | source)
XLA Modules:
  0.0 255.1 jit_solution(17460790023405655798)
XLA Ops:
  6.5 1.2 dynamic-slice_bitcast_fusion
  7.8 0.7 copy-done.2
  8.5 0.6 pad_maximum_fusion.3
  9.1 3.4 %collective-permute-start = (bf16[2,128,128]{2,1,0:T(8,128)(2,1)}, bf16[2,128,128]{2,1,0:T(8,128)(2,1)S(1)}, u32[]{:S(2)}, u32[]{:S(2)}) collective-permute-start(bf16[2,128,128]{2,1,0:T(8,128)(2,1)} %get-tuple-element.10), channel_id=1, source_target_pairs={{0,8},{8,16},{16,24},{1,9},{9,17},{17,25},{2,10},{10,18},{18,26},{... | collective-permute-start | bytes 196616 | tf_op jit(solution)/shard_map/ppermute | solution.py:23
  12.5 1.3 collective-permute-start.1
  14.0 3.0 %fusion.6 = pred[8,128,384]{1,2,0:T(8,128)(4,1)} fusion(s32[8,384]{1,0:T(8,128)S(1)} %add_add_fusion, s32[8,128]{1,0:T(8,128)S(1)} %add_add_fusion.1, pred[8,384]{1,0:T(8,128)(4,1)S(1)} %get-tuple-element.13, pred[8,384]{1,0:T(8,128)(4,1)S(1)} %get-tuple-element.12), kind=kLoop, calls=%fused_computation.18 | loop fusion | flops 1966080 | bytes 415744 | tf_op jit(solution)/shard_map/and | solution.py:55
  17.0 2.0 reshape.151
  19.0 1.0 pad_maximum_fusion.1
  21.9 0.7 fusion.2
  22.7 1.1 fusion.9
  24.2 3.2 %convolution_convert_fusion = bf16[1024,2048]{1,0:T(8,128)(2,1)} fusion(bf16[256,2048]{1,0:T(8,128)(2,1)S(1)} %copy-done.4, bf16[32,8,8,128]{3,2,1,0:T(8,128)(2,1)S(1)} %bitcast.64), kind=kOutput, calls=%fused_computation.3 | convolution fusion | flops 1075838976 | bytes 5767168 | tf_op jit(solution)/shard_map/dot_general | solution.py:95
  28.5 49.4 %reduce-scatter.3.cloned.1.call-done = bf16[128,2048]{1,0:T(8,128)(2,1)} async-done(((bf16[1024,2048]{1,0:T(8,128)(2,1)}), bf16[128,2048]{1,0:T(8,128)(2,1)}) %reduce-scatter.3.cloned.1.call-update) | async-done | bytes 524304 | tf_op jit(solution)/shard_map/reduce_scatter | solution.py:94
  77.9 1.2 fusion.10
  79.1 1.6 fusion.14
  80.8 0.8 copy-done.1
  82.0 14.4 %all_to_all.15 = bf16[4,40,2048]{2,1,0:T(8,128)(2,1)} all-to-all(bf16[4,40,2048]{2,1,0:T(8,128)(2,1)S(1)} %bitcast.66), channel_id=1, replica_groups=mesh['sp'=4,'tp'=8] {'sp'}, dimensions={0} | all-to-all | bytes 1310720 | tf_op jit(solution)/shard_map/all_to_all | solution.py:133
  96.7 7.0 %all_to_all.16 = bf16[4,40,3]{1,2,0:T(4,128)(2,1)S(1)} all-to-all(bf16[4,40,3]{1,2,0:T(4,128)(2,1)S(1)} %copy.51), channel_id=1, replica_groups=mesh['sp'=4,'tp'=8] {'sp'}, dimensions={0} | all-to-all | bytes 1920 | tf_op jit(solution)/shard_map/all_to_all | solution.py:134
  103.8 12.9 %all_gather.7 = bf16[32,40,3]{1,2,0:T(4,128)(2,1)S(1)} all-gather(bf16[4,40,3]{1,2,0:T(4,128)(2,1)S(1)} %all_to_all.16), channel_id=1, replica_groups=mesh['sp'=4,'tp'=8] {'tp'}, dimensions={0}, use_global_device_ids=true | all-gather | bytes 8640 | tf_op jit(solution)/shard_map/all_gather | solution.py:138
  116.8 33.2 %all-gather.2.cloned.1.call-done = bf16[32,40,2048]{2,1,0:T(8,128)(2,1)} async-done(((bf16[4,40,2048]{2,1,0:T(8,128)(2,1)}), bf16[32,40,2048]{2,1,0:T(8,128)(2,1)}) %all-gather.2.cloned.1.call-update) | async-done | bytes 5242896 | tf_op jit(solution)/shard_map/all_gather | solution.py:137
  150.0 9.7 %fusion.37 = f32[1280,3,256]{2,0,1:T(8,128)} fusion(bf16[1280,2048,1]{1,0,2:T(8,128)(2,1)} %bitcast.67, bf16[3,2048,256]{2,1,0:T(8,128)(2,1)} %param.25), kind=kOutput, calls=%fused_computation.70 | convolution fusion | flops 4026531840 | bytes 12320768 | tf_op jit(solution)/shard_map/md,edh->meh/dot_general | solution.py:142
  159.7 14.6 %bitcast_convert_fusion = bf16[1280,2048]{1,0:T(8,128)(2,1)} fusion(bf16[3,256,2048]{2,1,0:T(8,128)(2,1)S(1)} %copy-done, bf16[1280,2048,1]{1,0,2:T(8,128)(2,1)} %bitcast.68, bf16[3,2048,256]{2,1,0:T(8,128)(2,1)} %param.26, f32[1280,3,256]{2,0,1:T(8,128)} %fusion.37, f32[1280,3]{0,1:T(4,128)S(1)} %reshape.157), kind=kOutput, calls=%fused_computation | convolution fusion | flops 8062566400 | bytes 20724736 | tf_op jit(solution)/shard_map/meh,ehd->md/dot_general | solution.py:145
  174.3 57.5 %reduce-scatter.5.cloned.1.call-done = bf16[4,40,2048]{2,1,0:T(8,128)(2,1)} async-done(((bf16[32,40,2048]{2,1,0:T(8,128)(2,1)}), bf16[4,40,2048]{2,1,0:T(8,128)(2,1)}) %reduce-scatter.5.cloned.1.call-update) | async-done | bytes 655376 | tf_op jit(solution)/shard_map/reduce_scatter | solution.py:146
  231.8 14.6 %all_to_all.17 = bf16[4,40,2048]{2,1,0:T(8,128)(2,1)S(1)} all-to-all(bf16[4,40,2048]{2,1,0:T(8,128)(2,1)} %reduce-scatter.5.cloned.1.call-done), channel_id=1, replica_groups=mesh['sp'=4,'tp'=8] {'sp'}, dimensions={0} | all-to-all | bytes 1310720 | tf_op jit(solution)/shard_map/all_to_all | solution.py:152
  246.4 2.2 fusion.3
  (54 shorter events, 4.4 us)
Async XLA Ops:
  6.5 153.2 %copy-start = (bf16[3,256,2048]{2,1,0:T(8,128)(2,1)S(1)}, bf16[3,256,2048]{2,1,0:T(8,128)(2,1)}, u32[]{:S(2)}) copy-start(bf16[3,256,2048]{2,1,0:T(8,128)(2,1)} %param.27) | copy-start | bytes 9437188
  6.5 71.4 %reduce-scatter.3.cloned.1.call-start = ((), (), s32[]{:S(2)}) async-start(), calls=%async_computation.5 | async-start | bytes 4718592 | tf_op jit(solution)/shard_map/reduce_scatter | solution.py:94
  7.8 0.7 copy-start.2
  9.1 9.9 %collective-permute-start = (bf16[2,128,128]{2,1,0:T(8,128)(2,1)}, bf16[2,128,128]{2,1,0:T(8,128)(2,1)S(1)}, u32[]{:S(2)}, u32[]{:S(2)}) collective-permute-start(bf16[2,128,128]{2,1,0:T(8,128)(2,1)} %get-tuple-element.10), channel_id=1, source_target_pairs={{0,8},{8,16},{16,24},{1,9},{9,17},{17,25},{2,10},{10,18},{18,26},{... | collective-permute-start | bytes 196616 | tf_op jit(solution)/shard_map/ppermute | solution.py:23
  12.5 6.5 %collective-permute-start.1 = (bf16[2,128,128]{2,1,0:T(8,128)(2,1)S(1)}, bf16[2,128,128]{2,1,0:T(8,128)(2,1)}, u32[]{:S(2)}, u32[]{:S(2)}) collective-permute-start(bf16[2,128,128]{2,1,0:T(8,128)(2,1)S(1)} %get-tuple-element.11), channel_id=1, source_target_pairs={{8,0},{16,8},{24,16},{9,1},{17,9},{25,17},{10,2},{18,10},{26,18},{... | collective-permute-start | bytes 196616 | tf_op jit(solution)/shard_map/ppermute | solution.py:26
  20.0 1.0 copy-start.3
  20.0 1.2 copy-start.5
  21.2 0.7 copy-start.9
  22.7 1.4 copy-start.4
  27.4 0.7 copy-start.8
  27.4 51.7 %copy-start.6 = (f32[2048]{0:T(1024)S(1)}, f32[2048]{0:T(1024)}, u32[]{:S(2)}) copy-start(f32[2048]{0:T(1024)} %param.20) | copy-start | bytes 24580
  27.4 54.1 %copy-start.7 = (f32[2048]{0:T(1024)S(1)}, f32[2048]{0:T(1024)}, u32[]{:S(2)}) copy-start(f32[2048]{0:T(1024)} %param.21) | copy-start | bytes 24580
  27.4 69.0 %copy-start.11 = (bf16[128,2]{0,1:T(2,128)(2,1)S(1)}, bf16[128,2]{0,1:T(2,128)(2,1)}, u32[]{:S(2)}) copy-start(bf16[128,2]{0,1:T(2,128)(2,1)} %param.24) | copy-start | bytes 1540
  27.5 69.0 %copy-start.10 = (s32[128,2]{0,1:T(2,128)S(1)}, s32[128,2]{0,1:T(2,128)}, u32[]{:S(2)}) copy-start(s32[128,2]{0,1:T(2,128)} %param.23) | copy-start | bytes 3076
  27.5 122.5 %all-gather.2.cloned.1.call-start = ((), (), s32[]{:S(2)}) async-start(), calls=%async_computation.6 | async-start | bytes 5898240 | tf_op jit(solution)/shard_map/all_gather | solution.py:137
  80.7 0.8 copy-start.1
  96.4 135.5 %reduce-scatter.5.cloned.1.call-start = ((), (), s32[]{:S(2)}) async-start(), calls=%async_computation.7 | async-start | bytes 5898240 | tf_op jit(solution)/shard_map/reduce_scatter | solution.py:146
Sparse Core Ops, SparseCore 0:
  27.6 50.2 reduce-scatter.2
  96.5 53.4 all-gather.1
  174.4 57.3 reduce-scatter.4
where the time goes:
time: 257 us; the launch traced here: 255 us
  waiting for transfers between devices  140 us (54%)
  blocking collectives  48.9 us (19%)
  matrix products  32 us (12%)
  between operations  13.3 us (5%)
  other arithmetic  9.2 us (4%)
  local copies, waits for them, and re-layouts  6.79 us (3%)
  starting transfers between devices  4.76 us (2%)
    reduce_scatter x1, waiting for transfers between devices, per_device(): lax.psum_scatter(partial_out.reshape(pooled_rows.shape).astype(jnp.bfloat...  57.5 us
    reduce_scatter x1, waiting for transfers between devices, per_device(): lax.psum_scatter(jnp.dot(attended, out_weight, preferred_element_type=jnp...  49.4 us
    all_gather x1, waiting for transfers between devices, per_device(): lax.all_gather(arrived_rows, 'tp', axis=0, tiled=True)  33.2 us
    dot_general x1, matrix products, per_device(): jnp.einsum('meh,ehd->md', hidden, down_weight, preferred_element_type=jnp...  14.6 us
    all_to_all x1, blocking collectives, per_device(): lax.all_to_all(summed, 'sp', split_axis=0, concat_axis=0, tiled=True)  14.6 us
    all_to_all x1, blocking collectives, per_device(): lax.all_to_all(send_rows, 'sp', split_axis=0, concat_axis=0, tiled=True)  14.4 us
    all_gather x1, blocking collectives, per_device(): lax.all_gather(arrived_gates, 'tp', axis=0, tiled=True)  12.9 us
    dot_general x1, matrix products, per_device(): jnp.einsum('md,edh->meh', flat_rows, gate_weight, preferred_element_type=...  9.71 us
  transfers between devices with their start and end apart: 5, of which 3 were waited for; matrix products, arithmetic and copies ran while one was open for 2% of the time, Pallas kernels for 0%

commit v1 on v0

--- a/solution.py
+++ b/solution.py
@@ -1,6 +1,10 @@
+import functools
+
 import jax
 import jax.numpy as jnp
 from jax import lax
+from jax.experimental import pallas as pl
+from jax.experimental.pallas import tpu as pltpu
 from jax.sharding import PartitionSpec as P
 
 HEADS = 16
@@ -70,6 +74,282 @@
         "nhqk,nkd->nqhd", weight, key_spans[1], preferred_element_type=jnp.float32
     ).astype(jnp.bfloat16)
     return attended.reshape(seq_rows, heads_dev * HEAD_DIM)
+
+
+CORES = 2
+LANES = 128
+VMEM_SPEC = pl.BlockSpec(memory_space=pltpu.VMEM)
+
+
+def places():
+    count = lax.axis_size("tp") // CORES
+    me = lax.axis_index("tp")
+    chip, core = me // CORES, lax.rem(me, CORES)
+    up = lax.rem(chip + 1, count) * CORES + core
+    down = lax.rem(chip + count - 1, count) * CORES + core
+    partner = chip * CORES + 1 - core
+    return count, chip, core, (up, down), partner
+
+
+def greet(neighbours, partner, peers):
+    barrier = pltpu.get_barrier_semaphore()
+    for target in (*neighbours, partner):
+        pl.semaphore_signal(barrier, inc=1, device_id={"tp": target})
+    for peer in peers:
+        pl.semaphore_signal(barrier, inc=1, device_id={"sp": peer})
+    pl.semaphore_wait(barrier, 3 + len(peers))
+
+
+def column_halves(width):
+    low = (width // LANES + 1) // 2 * LANES
+    return (pl.ds(0, low), pl.ds(low, width - low)), (low, width - low)
+
+
+def spread_kernel(send_ref, out_ref, own_sem, swap_send, swap_recv, ring_send, ring_recv, core_send, core_recv):
+    count, chip, core, neighbours, partner = places()
+    me = lax.axis_index("tp")
+    groups = lax.axis_size("sp")
+    group = lax.axis_index("sp")
+    order = [lax.rem(group + j, groups) for j in range(groups)]
+    greet(neighbours, partner, order[1:])
+    halves, _ = column_halves(out_ref.shape[3])
+
+    def swap(j):
+        return pltpu.make_async_remote_copy(
+            src_ref=send_ref.at[order[j]],
+            dst_ref=out_ref.at[me, group],
+            send_sem=swap_send.at[j],
+            recv_sem=swap_recv.at[j],
+            device_id={"sp": order[j]},
+        )
+
+    def ring(side, step, j, source):
+        place = out_ref.at[source, order[j], :, halves[side]]
+        return pltpu.make_async_remote_copy(
+            src_ref=place,
+            dst_ref=place,
+            send_sem=ring_send.at[side, step, j],
+            recv_sem=ring_recv.at[side, step, j],
+            device_id={"tp": neighbours[side]},
+        )
+
+    def across(side, step, j, source):
+        place = out_ref.at[source, order[j], :, halves[side]]
+        return pltpu.make_async_remote_copy(
+            src_ref=place,
+            dst_ref=place,
+            send_sem=core_send.at[side, step, j],
+            recv_sem=core_recv.at[side, step, j],
+            device_id={"tp": partner},
+        )
+
+    def origin(side, step):
+        shift = step if side == 1 else count - step
+        return lax.rem(chip + shift, count) * CORES + core
+
+    own = pltpu.make_async_copy(send_ref.at[group], out_ref.at[me, group], own_sem)
+    own.start()
+    for j in range(1, groups):
+        swap(j).start()
+    arrival = [0] + [groups - j for j in range(1, groups)]
+    for j in range(groups):
+        if j == 0:
+            own.wait()
+        else:
+            swap(arrival[j]).wait_recv()
+        for side in range(2):
+            ring(side, 0, j, me).start()
+            across(side, 0, j, me).start()
+    for step in range(1, count):
+        for j in range(groups):
+            for side in range(2):
+                source = origin(side, step)
+                ring(side, step - 1, j, source).wait_recv()
+                if step < count - 1:
+                    ring(side, step, j, source).start()
+                across(side, step, j, source).start()
+    for j in range(1, groups):
+        swap(j).wait_send()
+    for step in range(count):
+        for j in range(groups):
+            for side in range(2):
+                if step < count - 1:
+                    ring(side, step, j, me).wait_send()
+                across(side, step, j, me).wait()
+
+
+def spread(send_rows):
+    groups, capacity, width = send_rows.shape
+    total = lax.axis_size("tp")
+    count = total // CORES
+    sem = pltpu.SemaphoreType.DMA
+    return pl.pallas_call(
+        spread_kernel,
+        out_shape=jax.ShapeDtypeStruct((total, groups, capacity, width), send_rows.dtype),
+        in_specs=[VMEM_SPEC],
+        out_specs=VMEM_SPEC,
+        scratch_shapes=[
+            sem,
+            sem((groups,)),
+            sem((groups,)),
+            sem((2, count, groups)),
+            sem((2, count, groups)),
+            sem((2, count, groups)),
+            sem((2, count, groups)),
+        ],
+        compiler_params=pltpu.CompilerParams(collective_id=1, has_side_effects=True),
+        name="spread",
+    )(send_rows)
+
+
+def gather_sum_kernel(
+    home, part_ref, out_ref, pair0, pair1, hold0, hold1, got0, got1, done,
+    core_send, core_recv, ring_send, ring_recv, swap_send, swap_recv,
+):
+    count, chip, core, neighbours, partner = places()
+    pieces = part_ref.shape[1]
+    groups = lax.axis_size("sp")
+    group = lax.axis_index("sp")
+    if home:
+        order = [lax.rem(group + j, groups) for j in range(groups)]
+        order = order[1:] + order[:1]
+        peers = order[:-1]
+    else:
+        order = list(range(pieces))
+        peers = []
+    greet(neighbours, partner, peers)
+    halves, _ = column_halves(part_ref.shape[3])
+    pair, hold, got = (pair0, pair1), (hold0, hold1), (got0, got1)
+
+    def target(side, step):
+        shift = count - 1 - step if side == 0 else 1 + step
+        return lax.rem(chip + shift, count) * CORES
+
+    def across(side, step, j):
+        return pltpu.make_async_remote_copy(
+            src_ref=part_ref.at[target(side, step) + 1 - core, order[j], :, halves[side]],
+            dst_ref=pair[side].at[step, j],
+            send_sem=core_send.at[side, step, j],
+            recv_sem=core_recv.at[side, step, j],
+            device_id={"tp": partner},
+        )
+
+    def ring(side, step, j):
+        return pltpu.make_async_remote_copy(
+            src_ref=hold[side].at[step, j],
+            dst_ref=got[side].at[step, j],
+            send_sem=ring_send.at[side, step, j],
+            recv_sem=ring_recv.at[side, step, j],
+            device_id={"tp": neighbours[side]},
+        )
+
+    def swap(j):
+        return pltpu.make_async_remote_copy(
+            src_ref=done.at[j],
+            dst_ref=out_ref.at[group],
+            send_sem=swap_send.at[j],
+            recv_sem=swap_recv.at[j],
+            device_id={"sp": order[j]},
+        )
+
+    for step in range(count):
+        for j in range(pieces):
+            for side in range(2):
+                across(side, step, j).start()
+    for step in range(count):
+        for j in range(pieces):
+            for side in range(2):
+                across(side, step, j).wait_recv()
+                value = part_ref[target(side, step) + core, order[j], :, halves[side]].astype(
+                    jnp.float32
+                ) + pair[side][step, j].astype(jnp.float32)
+                if step > 0:
+                    ring(side, step - 1, j).wait_recv()
+                    value = value + got[side][step - 1, j].astype(jnp.float32)
+                if step < count - 1:
+                    hold[side][step, j] = value.astype(hold[side].dtype)
+                    ring(side, step, j).start()
+                elif home and j < pieces - 1:
+                    done[j, :, halves[side]] = value.astype(done.dtype)
+                else:
+                    out_ref[order[j], :, halves[side]] = value.astype(out_ref.dtype)
+            if home and step == count - 1 and j < pieces - 1:
+                swap(j).start()
+    for step in range(count):
+        for j in range(pieces):
+            for side in range(2):
+                across(side, step, j).wait_send()
+                if step < count - 1:
+                    ring(side, step, j).wait_send()
+    if home:
+        for j in range(pieces - 1):
+            swap(j).wait()
+
+
+def gather_sum(part, home, out_type, collective_id):
+    total, pieces, rows, width = part.shape
+    count = total // CORES
+    _, widths = column_halves(width)
+    sem = pltpu.SemaphoreType.DMA
+    kind = part.dtype
+    return pl.pallas_call(
+        functools.partial(gather_sum_kernel, home),
+        out_shape=jax.ShapeDtypeStruct((pieces, rows, width), out_type),
+        in_specs=[VMEM_SPEC],
+        out_specs=VMEM_SPEC,
+        scratch_shapes=[
+            *[pltpu.VMEM((count, pieces, rows, w), kind) for w in widths],
+            *[pltpu.VMEM((count, pieces, rows, w), kind) for w in widths],
+            *[pltpu.VMEM((count, pieces, rows, w), kind) for w in widths],
+            pltpu.VMEM((pieces, rows, width), kind),
+            *[sem((2, count, pieces)) for _ in range(4)],
+            sem((pieces,)),
+            sem((pieces,)),
+        ],
+        compiler_params=pltpu.CompilerParams(
+            collective_id=collective_id, has_side_effects=True
+        ),
+        name="home_sum" if home else "row_sum",
+    )(part)
+
+
+def experts_kernel(rows_ref, gate_ref, up_ref, down_ref, out_ref):
+    width = out_ref.shape[1]
+    rows = rows_ref[:, :width]
+    gates = rows_ref[:, width:].astype(jnp.float32)
+    hidden = []
+    for member in range(gate_ref.shape[0]):
+        gate_pre = jnp.dot(rows, gate_ref[member], preferred_element_type=jnp.float32)
+        up_pre = jnp.dot(rows, up_ref[member], preferred_element_type=jnp.float32)
+        value = gate_pre / (1.0 + jnp.exp(-gate_pre)) * up_pre * gates[:, member : member + 1]
+        hidden.append(value.astype(jnp.bfloat16))
+    out_ref[...] = jnp.dot(
+        jnp.concatenate(hidden, axis=1), down_ref[...], preferred_element_type=jnp.float32
+    ).astype(out_ref.dtype)
+
+
+def experts(rows, gate_weight, up_weight, down_weight, block):
+    total, padded = rows.shape
+    members, width, hidden = gate_weight.shape
+    return pl.pallas_call(
+        experts_kernel,
+        out_shape=jax.ShapeDtypeStruct((total, width), rows.dtype),
+        grid=(total // block,),
+        in_specs=[
+            pl.BlockSpec((block, padded), lambda i: (i, 0)),
+            pl.BlockSpec((members, width, hidden), lambda i: (0, 0, 0)),
+            pl.BlockSpec((members, width, hidden), lambda i: (0, 0, 0)),
+            pl.BlockSpec((members * hidden, width), lambda i: (0, 0)),
+        ],
+        out_specs=pl.BlockSpec((block, width), lambda i: (i, 0)),
+        compiler_params=pltpu.CompilerParams(vmem_limit_bytes=48 * 1024 * 1024),
+        cost_estimate=pl.CostEstimate(
+            flops=6 * total * width * members * hidden,
+            bytes_accessed=2 * total * (width + padded) + 6 * members * hidden * width,
+            transcendentals=total * members * hidden,
+        ),
+        name="experts",
+    )(rows, gate_weight, up_weight, down_weight.reshape(members * hidden, width))
 
 
 def per_device(
@@ -91,12 +371,12 @@
     attended = window_attention(queries, key_heads, value_heads, sink_logit)
     tok_rows = residual.shape[0]
     width = out_weight.shape[1]
-    projected = lax.psum_scatter(
-        jnp.dot(attended, out_weight, preferred_element_type=jnp.float32).astype(jnp.bfloat16),
-        "tp",
-        scatter_dimension=0,
-        tiled=True,
-    ).astype(jnp.float32)
+    parts = lax.axis_size("tp")
+    pieces = 4 if tok_rows % 64 == 0 else 1
+    product = jnp.dot(attended, out_weight, preferred_element_type=jnp.float32).astype(jnp.bfloat16)
+    projected = gather_sum(
+        product.reshape(parts, pieces, tok_rows // pieces, width), False, jnp.float32, 0
+    ).reshape(tok_rows, width)
     proj_scale = lax.rsqrt(jnp.mean(projected * projected, axis=1, keepdims=True) + EPS)
     mixed_rows = (residual.astype(jnp.float32) + mixer_gain * (projected * proj_scale)).astype(
         jnp.bfloat16
@@ -119,37 +399,19 @@
         * (route_member[:, :, None] == member_ids[None, None, :]).astype(jnp.float32),
         axis=1,
     ).astype(jnp.bfloat16)
+    tail = jnp.pad(token_gates, ((0, 0), (0, LANES - GROUP_EXPERTS)))
     send_rows = (
-        jnp.dot(placing, normed, preferred_element_type=jnp.float32)
+        jnp.dot(placing, jnp.concatenate([normed, tail], axis=1), preferred_element_type=jnp.float32)
         .astype(jnp.bfloat16)
-        .reshape(groups, capacity, width)
-    )
-    send_gates = (
-        jnp.dot(placing, token_gates, preferred_element_type=jnp.float32)
-        .astype(jnp.bfloat16)
-        .reshape(groups, capacity, GROUP_EXPERTS)
-    )
-    arrived_rows, arrived_gates = (
-        lax.all_to_all(send_rows, "sp", split_axis=0, concat_axis=0, tiled=True),
-        lax.all_to_all(send_gates, "sp", split_axis=0, concat_axis=0, tiled=True),
-    )
-    pooled_rows, pooled_gates = (
-        lax.all_gather(arrived_rows, "tp", axis=0, tiled=True),
-        lax.all_gather(arrived_gates, "tp", axis=0, tiled=True),
-    )
-    flat_rows = pooled_rows.reshape(-1, width)
-    flat_gates = pooled_gates.reshape(-1, GROUP_EXPERTS).astype(jnp.float32)
-    gate_pre = jnp.einsum("md,edh->meh", flat_rows, gate_weight, preferred_element_type=jnp.float32)
-    up_pre = jnp.einsum("md,edh->meh", flat_rows, up_weight, preferred_element_type=jnp.float32)
-    hidden = (jax.nn.silu(gate_pre) * up_pre * flat_gates[:, :, None]).astype(jnp.bfloat16)
-    partial_out = jnp.einsum("meh,ehd->md", hidden, down_weight, preferred_element_type=jnp.float32)
-    summed = lax.psum_scatter(
-        partial_out.reshape(pooled_rows.shape).astype(jnp.bfloat16),
-        "tp",
-        scatter_dimension=0,
-        tiled=True,
-    )
-    returned = lax.all_to_all(summed, "sp", split_axis=0, concat_axis=0, tiled=True)
+        .reshape(groups, capacity, width + LANES)
+    )
+    pooled = spread(send_rows)
+    partial_out = experts(
+        pooled.reshape(-1, width + LANES), gate_weight, up_weight, down_weight, 2 * groups * capacity
+    )
+    returned = gather_sum(
+        partial_out.reshape(parts, groups, capacity, width), True, jnp.bfloat16, 2
+    )
     expert_out = lax.dot_general(
         placing,
         returned.reshape(groups * capacity, width),

time: 257 us -> 208 us (0.81)
  Pallas kernels: 0 us -> 177 us
  waiting for transfers between devices: 140 us -> 0.01 us
  blocking collectives: 48.9 us -> 0 us
  matrix products: 32 us -> 8.38 us
  between operations: 13.3 us -> 0.21 us
    pallas_call x0 -> x4, Pallas kernels: none -> 177 us  [the longest x2 96.8 us: gather_sum(): pl.pallas_call(functools.partial(gather_sum_kernel, home), out_shape=jax....]
    reduce_scatter x2 -> x0, waiting for transfers between devices: 107 us -> none  [the longest x1 57.5 us: per_device(): lax.psum_scatter(partial_out.reshape(pooled_rows.shape).astype(jnp.bfloat...]
    all_to_all x3 -> x0, blocking collectives: 36 us -> none  [the longest x1 14.6 us: per_device(): lax.all_to_all(summed, 'sp', split_axis=0, concat_axis=0, tiled=True)]
    all_gather x1 -> x0, waiting for transfers between devices: 33.2 us -> none  [per_device(): lax.all_gather(arrived_rows, 'tp', axis=0, tiled=True)]
    dot_general x4 -> x1, matrix products: 24.9 us -> 1.22 us  [per_device(): jnp.dot(placing, jnp.concatenate([normed, tail], axis=1), preferred_eleme...]
    all_gather x1 -> x0, blocking collectives: 12.9 us -> none  [per_device(): lax.all_gather(arrived_gates, 'tp', axis=0, tiled=True)]
  transfers between devices with their start and end apart: 5 -> 2, of which waited for: 3 -> 0; matrix products, arithmetic and copies ran while one was open for 2% -> 3% of each run, Pallas kernels for 0% -> 0%
where the time goes in v1:
time: 208 us; the launch traced here: 206 us
  Pallas kernels  177 us (85%)
  other arithmetic  10.1 us (5%)
  matrix products  8.38 us (4%)
  local copies, waits for them, and re-layouts  5.16 us (2%)
  starting transfers between devices  4.69 us (2%)
    pallas_call x2, Pallas kernels, gather_sum(): pl.pallas_call(functools.partial(gather_sum_kernel, home), out_shape=jax....  96.8 us
    pallas_call x1, Pallas kernels, spread(): pl.pallas_call(spread_kernel, out_shape=jax.ShapeDtypeStruct((total, grou...  63 us
    pallas_call x1, Pallas kernels, experts(): pl.pallas_call(experts_kernel, out_shape=jax.ShapeDtypeStruct((total, wid...  17.4 us
  transfers between devices with their start and end apart: 2, of which 0 were waited for; matrix products, arithmetic and copies ran while one was open for 3% of the time, Pallas kernels for 0%

profile of v1, /device:TPU:16, one launch (start us, length us, event | category | flops | bytes accessed | tf_op | source)
XLA Modules:
  0.0 205.7 jit_solution(4345059636989611395)
XLA Ops:
  0.0 1.2 dynamic-slice_bitcast_fusion
  1.2 3.4 %collective-permute-start = (bf16[2,128,128]{2,1,0:T(8,128)(2,1)S(1)}, bf16[2,128,128]{2,1,0:T(8,128)(2,1)S(1)}, u32[]{:S(2)}, u32[]{:S(2)}) collective-permute-start(bf16[2,128,128]{2,1,0:T(8,128)(2,1)S(1)} %get-tuple-element.10), channel_id=1, source_target_pairs={{0,8},{8,16},{16,24},{1,9},{9,17},{17,25},{2,10},{10,18},{18,26},{... | collective-permute-start | bytes 196616 | tf_op jit(solution)/shard_map/ppermute | solution.py:27
  4.6 1.3 collective-permute-start.1
  6.1 0.7 convert_element_type.52
  6.7 0.7 fusion.25
  7.6 0.8 select_reduce_fusion
  8.5 0.7 multiply_add_fusion
  9.1 1.9 fusion.4
  11.0 0.7 fusion.30
  11.8 1.2 reshape.159
  13.1 0.4 fusion.37
  13.6 0.6 fusion.2
  14.3 0.8 fusion
  15.2 1.1 fusion.7
  16.6 3.2 %convolution_convert_fusion = bf16[1024,2048]{1,0:T(8,128)(2,1)} fusion(bf16[256,2048]{1,0:T(8,128)(2,1)S(1)} %copy-done, bf16[32,8,8,128]{3,2,1,0:T(8,128)(2,1)S(1)} %bitcast.63), kind=kOutput, calls=%fused_computation | convolution fusion | flops 1075838976 | bytes 5767168 | tf_op jit(solution)/shard_map/dot_general | solution.py:376
  19.9 42.4 %row_sum.1 = f32[4,32,2048]{2,1,0:T(8,128)} custom-call(bf16[8,4,32,2048]{3,2,1,0:T(8,128)(2,1)} %bitcast.59), custom_call_target="tpu_custom_call" | custom-call | tf_op jit(solution)/shard_map/row_sum/pallas_call | solution.py:295
  62.3 1.4 multiply_reduce_fusion
  63.8 1.6 fusion.9
  65.6 1.2 convolution_convert_fusion.1
  66.8 63.0 %spread.1 = bf16[8,4,40,2176]{3,2,1,0:T(8,128)(2,1)} custom-call(bf16[4,40,2176]{2,1,0:T(8,128)(2,1)} %bitcast.65), custom_call_target="tpu_custom_call" | custom-call | tf_op jit(solution)/shard_map/spread/pallas_call | solution.py:186
  129.8 1.9 copy-done.1
  131.7 17.4 %experts.1 = bf16[1280,2048]{1,0:T(8,128)(2,1)} custom-call(bf16[1280,2176]{1,0:T(8,128)(2,1)} %bitcast.61, bf16[3,2048,256]{2,1,0:T(8,128)(2,1)S(1)} %copy-done.1, bf16[3,2048,256]{2,1,0:T(8,128)(2,1)} %up_ref.1, bf16[768,2048]{1,0:T(8,128)(2,1)} %bitcast.66), custom_call_target="tpu_custom_call" | custom-call | flops 12079595520 | bytes 20250624 | tf_op jit(solution)/shard_map/experts/pallas_call | solution.py:334
  149.1 54.4 %home_sum.1 = bf16[4,40,2048]{2,1,0:T(8,128)(2,1)} custom-call(bf16[8,4,40,2048]{3,2,1,0:T(8,128)(2,1)} %bitcast.62), custom_call_target="tpu_custom_call" | custom-call | tf_op jit(solution)/shard_map/home_sum/pallas_call | solution.py:295
  203.4 2.2 %fusion.1 = bf16[128,2048]{1,0:T(8,128)(2,1)} fusion(bf16[160,2048]{1,0:T(8,128)(2,1)} %bitcast.64, bf16[128,2048]{1,0:T(8,128)(2,1)S(1)} %get-tuple-element.6, s32[128]{0:T(128)S(1)} %multiply_add_fusion), kind=kOutput, calls=%fused_computation.7 | convolution fusion | flops 84692992 | bytes 1704448 | tf_op jit(solution)/shard_map/dot_general | solution.py:415
  (29 shorter events, 1.5 us)
Async XLA Ops:
  0.0 16.6 %copy-start = (bf16[256,2048]{1,0:T(8,128)(2,1)S(1)}, bf16[256,2048]{1,0:T(8,128)(2,1)}, u32[]{:S(2)}) copy-start(bf16[256,2048]{1,0:T(8,128)(2,1)} %param.18) | copy-start | bytes 3145732
  1.2 11.8 %collective-permute-start = (bf16[2,128,128]{2,1,0:T(8,128)(2,1)S(1)}, bf16[2,128,128]{2,1,0:T(8,128)(2,1)S(1)}, u32[]{:S(2)}, u32[]{:S(2)}) collective-permute-start(bf16[2,128,128]{2,1,0:T(8,128)(2,1)S(1)} %get-tuple-element.10), channel_id=1, source_target_pairs={{0,8},{8,16},{16,24},{1,9},{9,17},{17,25},{2,10},{10,18},{18,26},{... | collective-permute-start | bytes 196616 | tf_op jit(solution)/shard_map/ppermute | solution.py:27
  4.6 8.4 %collective-permute-start.1 = (bf16[2,128,128]{2,1,0:T(8,128)(2,1)S(1)}, bf16[2,128,128]{2,1,0:T(8,128)(2,1)S(1)}, u32[]{:S(2)}, u32[]{:S(2)}) collective-permute-start(bf16[2,128,128]{2,1,0:T(8,128)(2,1)S(1)} %get-tuple-element.11), channel_id=1, source_target_pairs={{8,0},{16,8},{24,16},{9,1},{17,9},{25,17},{10,2},{18,10},{26,18},{... | collective-permute-start | bytes 196616 | tf_op jit(solution)/shard_map/ppermute | solution.py:30
  13.6 0.7 copy-start.5
  19.8 43.9 %copy-start.2 = (bf16[128,2048]{1,0:T(8,128)(2,1)S(1)}, bf16[128,2048]{1,0:T(8,128)(2,1)}, u32[]{:S(2)}) copy-start(bf16[128,2048]{1,0:T(8,128)(2,1)} %param.19) | copy-start | bytes 1572868
  19.8 43.9 %copy-start.3 = (f32[2048]{0:T(1024)S(1)}, f32[2048]{0:T(1024)}, u32[]{:S(2)}) copy-start(f32[2048]{0:T(1024)} %param.20) | copy-start | bytes 24580
  19.9 45.5 %copy-start.4 = (f32[2048]{0:T(1024)S(1)}, f32[2048]{0:T(1024)}, u32[]{:S(2)}) copy-start(f32[2048]{0:T(1024)} %param.21) | copy-start | bytes 24580
  129.8 1.9 copy-start.1

commit v2 on v1

--- a/solution.py
+++ b/solution.py
@@ -100,19 +100,13 @@
     pl.semaphore_wait(barrier, 3 + len(peers))
 
 
-def column_halves(width):
-    low = (width // LANES + 1) // 2 * LANES
-    return (pl.ds(0, low), pl.ds(low, width - low)), (low, width - low)
-
-
-def spread_kernel(send_ref, out_ref, own_sem, swap_send, swap_recv, ring_send, ring_recv, core_send, core_recv):
+def spread_kernel(send_ref, out_ref, own_sem, swap_send, swap_recv, line_send, line_recv, core_send, core_recv):
     count, chip, core, neighbours, partner = places()
     me = lax.axis_index("tp")
     groups = lax.axis_size("sp")
     group = lax.axis_index("sp")
     order = [lax.rem(group + j, groups) for j in range(groups)]
     greet(neighbours, partner, order[1:])
-    halves, _ = column_halves(out_ref.shape[3])
 
     def swap(j):
         return pltpu.make_async_remote_copy(
@@ -123,18 +117,18 @@
             device_id={"sp": order[j]},
         )
 
-    def ring(side, step, j, source):
-        place = out_ref.at[source, order[j], :, halves[side]]
+    def line(side, step, j, source):
+        place = out_ref.at[source, order[j]]
         return pltpu.make_async_remote_copy(
             src_ref=place,
             dst_ref=place,
-            send_sem=ring_send.at[side, step, j],
-            recv_sem=ring_recv.at[side, step, j],
+            send_sem=line_send.at[side, step, j],
+            recv_sem=line_recv.at[side, step, j],
             device_id={"tp": neighbours[side]},
         )
 
     def across(side, step, j, source):
-        place = out_ref.at[source, order[j], :, halves[side]]
+        place = out_ref.at[source, order[j]]
         return pltpu.make_async_remote_copy(
             src_ref=place,
             dst_ref=place,
@@ -143,39 +137,63 @@
             device_id={"tp": partner},
         )
 
+    def behind(side, step):
+        return chip >= step if side == 0 else chip + step < count
+
     def origin(side, step):
-        shift = step if side == 1 else count - step
-        return lax.rem(chip + shift, count) * CORES + core
-
+        return (chip - step if side == 0 else chip + step) * CORES + core
+
+    ahead = (chip + 1 < count, chip >= 1)
     own = pltpu.make_async_copy(send_ref.at[group], out_ref.at[me, group], own_sem)
     own.start()
     for j in range(1, groups):
         swap(j).start()
-    arrival = [0] + [groups - j for j in range(1, groups)]
     for j in range(groups):
         if j == 0:
             own.wait()
         else:
-            swap(arrival[j]).wait_recv()
+            swap(groups - j).wait_recv()
         for side in range(2):
-            ring(side, 0, j, me).start()
-            across(side, 0, j, me).start()
+
+            @pl.when(ahead[side])
+            def _():
+                line(side, 0, j, me).start()
+
+        across(0, 0, j, me).start()
     for step in range(1, count):
         for j in range(groups):
             for side in range(2):
-                source = origin(side, step)
-                ring(side, step - 1, j, source).wait_recv()
-                if step < count - 1:
-                    ring(side, step, j, source).start()
-                across(side, step, j, source).start()
+
+                @pl.when(behind(side, step))
+                def _():
+                    source = origin(side, step)
+                    line(side, step - 1, j, source).wait_recv()
+                    if step < count - 1:
+
+                        @pl.when(ahead[side])
+                        def _():
+                            line(side, step, j, source).start()
+
+                    across(side, step, j, source).start()
+
     for j in range(1, groups):
         swap(j).wait_send()
+    for j in range(groups):
+        across(0, 0, j, me).wait()
     for step in range(count):
         for j in range(groups):
             for side in range(2):
                 if step < count - 1:
-                    ring(side, step, j, me).wait_send()
-                across(side, step, j, me).wait()
+
+                    @pl.when(behind(side, step) & ahead[side])
+                    def _():
+                        line(side, step, j, me).wait_send()
+
+                if step > 0:
+
+                    @pl.when(behind(side, step))
+                    def _():
+                        across(side, step, j, me).wait()
 
 
 def spread(send_rows):
@@ -203,8 +221,8 @@
 
 
 def gather_sum_kernel(
-    home, part_ref, out_ref, pair0, pair1, hold0, hold1, got0, got1, done,
-    core_send, core_recv, ring_send, ring_recv, swap_send, swap_recv,
+    home, part_ref, out_ref, pair, got, done, final,
+    core_send, core_recv, line_send, line_recv, swap_send, swap_recv,
 ):
     count, chip, core, neighbours, partner = places()
     pieces = part_ref.shape[1]
@@ -218,28 +236,22 @@
         order = list(range(pieces))
         peers = []
     greet(neighbours, partner, peers)
-    halves, _ = column_halves(part_ref.shape[3])
-    pair, hold, got = (pair0, pair1), (hold0, hold1), (got0, got1)
-
-    def target(side, step):
-        shift = count - 1 - step if side == 0 else 1 + step
-        return lax.rem(chip + shift, count) * CORES
-
-    def across(side, step, j):
-        return pltpu.make_async_remote_copy(
-            src_ref=part_ref.at[target(side, step) + 1 - core, order[j], :, halves[side]],
-            dst_ref=pair[side].at[step, j],
-            send_sem=core_send.at[side, step, j],
-            recv_sem=core_recv.at[side, step, j],
+
+    def across(dest, j):
+        return pltpu.make_async_remote_copy(
+            src_ref=part_ref.at[dest * CORES + 1 - core, order[j]],
+            dst_ref=pair.at[dest, j],
+            send_sem=core_send.at[dest, j],
+            recv_sem=core_recv.at[dest, j],
             device_id={"tp": partner},
         )
 
-    def ring(side, step, j):
-        return pltpu.make_async_remote_copy(
-            src_ref=hold[side].at[step, j],
-            dst_ref=got[side].at[step, j],
-            send_sem=ring_send.at[side, step, j],
-            recv_sem=ring_recv.at[side, step, j],
+    def line(side, dest, j):
+        return pltpu.make_async_remote_copy(
+            src_ref=pair.at[dest, j],
+            dst_ref=got.at[side, dest, j],
+            send_sem=line_send.at[side, dest, j],
+            recv_sem=line_recv.at[side, dest, j],
             device_id={"tp": neighbours[side]},
         )
 
@@ -252,35 +264,68 @@
             device_id={"sp": order[j]},
         )
 
-    for step in range(count):
+    def local(dest, j):
+        across(dest, j).wait_recv()
+        return part_ref[dest * CORES + core, order[j]].astype(jnp.float32) + pair[
+            dest, j
+        ].astype(jnp.float32)
+
+    sends = []
+    for step in range(count - 1):
+        sends += [(0, count - 1 - step), (1, step)]
+    first = []
+    for _, dest in sends:
+        if dest not in first:
+            first.append(dest)
+    for dest in first:
         for j in range(pieces):
-            for side in range(2):
-                across(side, step, j).start()
-    for step in range(count):
+            across(dest, j).start()
+    start = (chip == 0, chip == count - 1)
+    inside = (chip > 0, chip < count - 1)
+    for step in range(count - 1):
         for j in range(pieces):
-            for side in range(2):
-                across(side, step, j).wait_recv()
-                value = part_ref[target(side, step) + core, order[j], :, halves[side]].astype(
-                    jnp.float32
-                ) + pair[side][step, j].astype(jnp.float32)
-                if step > 0:
-                    ring(side, step - 1, j).wait_recv()
-                    value = value + got[side][step - 1, j].astype(jnp.float32)
-                if step < count - 1:
-                    hold[side][step, j] = value.astype(hold[side].dtype)
-                    ring(side, step, j).start()
-                elif home and j < pieces - 1:
-                    done[j, :, halves[side]] = value.astype(done.dtype)
-                else:
-                    out_ref[order[j], :, halves[side]] = value.astype(out_ref.dtype)
-            if home and step == count - 1 and j < pieces - 1:
-                swap(j).start()
-    for step in range(count):
-        for j in range(pieces):
-            for side in range(2):
-                across(side, step, j).wait_send()
-                if step < count - 1:
-                    ring(side, step, j).wait_send()
+            for side, dest in sends[2 * step : 2 * step + 2]:
+                toward = chip < dest if side == 0 else chip > dest
+
+                @pl.when(start[side])
+                def _():
+                    pair[dest, j] = local(dest, j).astype(pair.dtype)
+
+                @pl.when(inside[side] & toward)
+                def _():
+                    value = local(dest, j)
+                    line(side, dest, j).wait_recv()
+                    pair[dest, j] = (value + got[side, dest, j].astype(jnp.float32)).astype(
+                        pair.dtype
+                    )
+
+                @pl.when(toward)
+                def _():
+                    line(side, dest, j).start()
+
+    for j in range(pieces):
+        final[...] = local(chip, j)
+        for side in range(2):
+
+            @pl.when(inside[side])
+            def _():
+                line(side, chip, j).wait_recv()
+                final[...] += got[side, chip, j].astype(jnp.float32)
+
+        if home and j < pieces - 1:
+            done[j] = final[...].astype(done.dtype)
+            swap(j).start()
+        else:
+            out_ref[order[j]] = final[...].astype(out_ref.dtype)
+    for j in range(pieces):
+        for dest in range(count):
+            across(dest, j).wait_send()
+        for side, dest in sends:
+
+            @pl.when(chip < dest if side == 0 else chip > dest)
+            def _():
+                line(side, dest, j).wait_send()
+
     if home:
         for j in range(pieces - 1):
             swap(j).wait()
@@ -289,7 +334,6 @@
 def gather_sum(part, home, out_type, collective_id):
     total, pieces, rows, width = part.shape
     count = total // CORES
-    _, widths = column_halves(width)
     sem = pltpu.SemaphoreType.DMA
     kind = part.dtype
     return pl.pallas_call(
@@ -298,11 +342,14 @@
         in_specs=[VMEM_SPEC],
         out_specs=VMEM_SPEC,
         scratch_shapes=[
-            *[pltpu.VMEM((count, pieces, rows, w), kind) for w in widths],
-            *[pltpu.VMEM((count, pieces, rows, w), kind) for w in widths],
-            *[pltpu.VMEM((count, pieces, rows, w), kind) for w in widths],
+            pltpu.VMEM((count, pieces, rows, width), kind),
+            pltpu.VMEM((2, count, pieces, rows, width), kind),
             pltpu.VMEM((pieces, rows, width), kind),
-            *[sem((2, count, pieces)) for _ in range(4)],
+            pltpu.VMEM((rows, width), jnp.float32),
+            sem((count, pieces)),
+            sem((count, pieces)),
+            sem((2, count, pieces)),
+            sem((2, count, pieces)),
             sem((pieces,)),
             sem((pieces,)),
         ],

time: 208 us -> 228 us (1.096)
  Pallas kernels: 177 us -> 199 us
    pallas_call x2, Pallas kernels: 96.8 us -> 125 us  [gather_sum(): pl.pallas_call(functools.partial(gather_sum_kernel, home), out_shape=jax....]
    pallas_call x1, Pallas kernels: 63 us -> 56.6 us  [spread(): pl.pallas_call(spread_kernel, out_shape=jax.ShapeDtypeStruct((total, grou...]
where the time goes in v2:
time: 228 us; the launch traced here: 227 us
  Pallas kernels  199 us (87%)
  other arithmetic  10.1 us (4%)
  matrix products  8.37 us (4%)
  local copies, waits for them, and re-layouts  5.17 us (2%)
  starting transfers between devices  4.69 us (2%)
    pallas_call x2, Pallas kernels, gather_sum(): pl.pallas_call(functools.partial(gather_sum_kernel, home), out_shape=jax....  125 us
    pallas_call x1, Pallas kernels, spread(): pl.pallas_call(spread_kernel, out_shape=jax.ShapeDtypeStruct((total, grou...  56.6 us
    pallas_call x1, Pallas kernels, experts(): pl.pallas_call(experts_kernel, out_shape=jax.ShapeDtypeStruct((total, wid...  17.4 us
  transfers between devices with their start and end apart: 2, of which 0 were waited for; matrix products, arithmetic and copies ran while one was open for 3% of the time, Pallas kernels for 0%

profile of v2, /device:TPU:16, one launch (start us, length us, event | category | flops | bytes accessed | tf_op | source)
XLA Modules:
  0.0 227.3 jit_solution(9899369561103533)
XLA Ops:
  0.0 1.2 dynamic-slice_bitcast_fusion
  1.2 3.4 %collective-permute-start = (bf16[2,128,128]{2,1,0:T(8,128)(2,1)S(1)}, bf16[2,128,128]{2,1,0:T(8,128)(2,1)S(1)}, u32[]{:S(2)}, u32[]{:S(2)}) collective-permute-start(bf16[2,128,128]{2,1,0:T(8,128)(2,1)S(1)} %get-tuple-element.10), channel_id=1, source_target_pairs={{0,8},{8,16},{16,24},{1,9},{9,17},{17,25},{2,10},{10,18},{18,26},{... | collective-permute-start | bytes 196616 | tf_op jit(solution)/shard_map/ppermute | solution.py:27
  4.6 1.3 collective-permute-start.1
  6.1 0.7 convert_element_type.52
  6.7 0.7 fusion.25
  7.6 0.8 select_reduce_fusion
  8.5 0.7 multiply_add_fusion
  9.1 1.9 fusion.4
  11.0 0.7 fusion.30
  11.8 1.2 reshape.159
  13.1 0.4 fusion.37
  13.6 0.6 fusion.2
  14.3 0.8 fusion
  15.2 1.1 fusion.7
  16.6 3.2 %convolution_convert_fusion = bf16[1024,2048]{1,0:T(8,128)(2,1)} fusion(bf16[256,2048]{1,0:T(8,128)(2,1)S(1)} %copy-done, bf16[32,8,8,128]{3,2,1,0:T(8,128)(2,1)S(1)} %bitcast.63), kind=kOutput, calls=%fused_computation | convolution fusion | flops 1075838976 | bytes 5767168 | tf_op jit(solution)/shard_map/dot_general | solution.py:423
  19.9 57.1 %row_sum.1 = f32[4,32,2048]{2,1,0:T(8,128)} custom-call(bf16[8,4,32,2048]{3,2,1,0:T(8,128)(2,1)} %bitcast.59), custom_call_target="tpu_custom_call" | custom-call | tf_op jit(solution)/shard_map/row_sum/pallas_call | solution.py:339
  77.0 1.4 multiply_reduce_fusion
  78.4 1.6 fusion.9
  80.3 1.2 convolution_convert_fusion.1
  81.5 56.6 %spread.1 = bf16[8,4,40,2176]{3,2,1,0:T(8,128)(2,1)} custom-call(bf16[4,40,2176]{2,1,0:T(8,128)(2,1)} %bitcast.65), custom_call_target="tpu_custom_call" | custom-call | tf_op jit(solution)/shard_map/spread/pallas_call | solution.py:204
  138.1 1.9 copy-done.1
  140.0 17.4 %experts.1 = bf16[1280,2048]{1,0:T(8,128)(2,1)} custom-call(bf16[1280,2176]{1,0:T(8,128)(2,1)} %bitcast.61, bf16[3,2048,256]{2,1,0:T(8,128)(2,1)S(1)} %copy-done.1, bf16[3,2048,256]{2,1,0:T(8,128)(2,1)} %up_ref.1, bf16[768,2048]{1,0:T(8,128)(2,1)} %bitcast.66), custom_call_target="tpu_custom_call" | custom-call | flops 12079595520 | bytes 20250624 | tf_op jit(solution)/shard_map/experts/pallas_call | solution.py:381
  157.3 67.7 %home_sum.1 = bf16[4,40,2048]{2,1,0:T(8,128)(2,1)} custom-call(bf16[8,4,40,2048]{3,2,1,0:T(8,128)(2,1)} %bitcast.62), custom_call_target="tpu_custom_call" | custom-call | tf_op jit(solution)/shard_map/home_sum/pallas_call | solution.py:339
  225.1 2.2 fusion.1
  (29 shorter events, 1.5 us)
Async XLA Ops:
  0.0 16.6 %copy-start = (bf16[256,2048]{1,0:T(8,128)(2,1)S(1)}, bf16[256,2048]{1,0:T(8,128)(2,1)}, u32[]{:S(2)}) copy-start(bf16[256,2048]{1,0:T(8,128)(2,1)} %param.18) | copy-start | bytes 3145732
  1.2 11.8 %collective-permute-start = (bf16[2,128,128]{2,1,0:T(8,128)(2,1)S(1)}, bf16[2,128,128]{2,1,0:T(8,128)(2,1)S(1)}, u32[]{:S(2)}, u32[]{:S(2)}) collective-permute-start(bf16[2,128,128]{2,1,0:T(8,128)(2,1)S(1)} %get-tuple-element.10), channel_id=1, source_target_pairs={{0,8},{8,16},{16,24},{1,9},{9,17},{17,25},{2,10},{10,18},{18,26},{... | collective-permute-start | bytes 196616 | tf_op jit(solution)/shard_map/ppermute | solution.py:27
  4.6 8.4 %collective-permute-start.1 = (bf16[2,128,128]{2,1,0:T(8,128)(2,1)S(1)}, bf16[2,128,128]{2,1,0:T(8,128)(2,1)S(1)}, u32[]{:S(2)}, u32[]{:S(2)}) collective-permute-start(bf16[2,128,128]{2,1,0:T(8,128)(2,1)S(1)} %get-tuple-element.11), channel_id=1, source_target_pairs={{8,0},{16,8},{24,16},{9,1},{17,9},{25,17},{10,2},{18,10},{26,18},{... | collective-permute-start | bytes 196616 | tf_op jit(solution)/shard_map/ppermute | solution.py:30
  13.6 0.7 copy-start.5
  19.8 58.6 %copy-start.2 = (bf16[128,2048]{1,0:T(8,128)(2,1)S(1)}, bf16[128,2048]{1,0:T(8,128)(2,1)}, u32[]{:S(2)}) copy-start(bf16[128,2048]{1,0:T(8,128)(2,1)} %param.19) | copy-start | bytes 1572868
  19.8 58.6 %copy-start.3 = (f32[2048]{0:T(1024)S(1)}, f32[2048]{0:T(1024)}, u32[]{:S(2)}) copy-start(f32[2048]{0:T(1024)} %param.20) | copy-start | bytes 24580
  19.9 60.2 %copy-start.4 = (f32[2048]{0:T(1024)S(1)}, f32[2048]{0:T(1024)}, u32[]{:S(2)}) copy-start(f32[2048]{0:T(1024)} %param.21) | copy-start | bytes 24580
  138.1 1.9 copy-start.1

commit v3 on v1

--- a/solution.py
+++ b/solution.py
@@ -372,7 +372,7 @@
     tok_rows = residual.shape[0]
     width = out_weight.shape[1]
     parts = lax.axis_size("tp")
-    pieces = 4 if tok_rows % 64 == 0 else 1
+    pieces = 8 if tok_rows % 128 == 0 else 1
     product = jnp.dot(attended, out_weight, preferred_element_type=jnp.float32).astype(jnp.bfloat16)
     projected = gather_sum(
         product.reshape(parts, pieces, tok_rows // pieces, width), False, jnp.float32, 0

time: 208 us -> 209 us (level)
  no operation moved by 1% of the time
where the time goes in v3:
time: 209 us; the launch traced here: 207 us
  Pallas kernels  179 us (86%)
  other arithmetic  10.1 us (5%)
  matrix products  8.38 us (4%)
  local copies, waits for them, and re-layouts  5.16 us (2%)
  starting transfers between devices  4.69 us (2%)
    pallas_call x2, Pallas kernels, gather_sum(): pl.pallas_call(functools.partial(gather_sum_kernel, home), out_shape=jax....  97.6 us
    pallas_call x1, Pallas kernels, spread(): pl.pallas_call(spread_kernel, out_shape=jax.ShapeDtypeStruct((total, grou...  63.6 us
    pallas_call x1, Pallas kernels, experts(): pl.pallas_call(experts_kernel, out_shape=jax.ShapeDtypeStruct((total, wid...  17.4 us
  transfers between devices with their start and end apart: 2, of which 0 were waited for; matrix products, arithmetic and copies ran while one was open for 3% of the time, Pallas kernels for 0%

profile of v3, /device:TPU:16, one launch (start us, length us, event | category | flops | bytes accessed | tf_op | source)
XLA Modules:
  0.0 207.1 jit_solution(3913200907212596417)
XLA Ops:
  0.0 1.2 dynamic-slice_bitcast_fusion
  1.2 3.4 %collective-permute-start = (bf16[2,128,128]{2,1,0:T(8,128)(2,1)S(1)}, bf16[2,128,128]{2,1,0:T(8,128)(2,1)S(1)}, u32[]{:S(2)}, u32[]{:S(2)}) collective-permute-start(bf16[2,128,128]{2,1,0:T(8,128)(2,1)S(1)} %get-tuple-element.10), channel_id=1, source_target_pairs={{0,8},{8,16},{16,24},{1,9},{9,17},{17,25},{2,10},{10,18},{18,26},{... | collective-permute-start | bytes 196616 | tf_op jit(solution)/shard_map/ppermute | solution.py:27
  4.6 1.3 collective-permute-start.1
  6.1 0.7 convert_element_type.52
  6.7 0.7 fusion.25
  7.6 0.8 select_reduce_fusion
  8.5 0.7 multiply_add_fusion
  9.1 1.9 fusion.4
  11.0 0.7 fusion.30
  11.8 1.2 reshape.159
  13.1 0.4 fusion.37
  13.6 0.6 fusion.2
  14.3 0.8 fusion
  15.2 1.1 fusion.7
  16.6 3.2 %convolution_convert_fusion = bf16[1024,2048]{1,0:T(8,128)(2,1)} fusion(bf16[256,2048]{1,0:T(8,128)(2,1)S(1)} %copy-done, bf16[32,8,8,128]{3,2,1,0:T(8,128)(2,1)S(1)} %bitcast.63), kind=kOutput, calls=%fused_computation | convolution fusion | flops 1075838976 | bytes 5767168 | tf_op jit(solution)/shard_map/dot_general | solution.py:376
  19.9 43.6 %row_sum.1 = f32[8,16,2048]{2,1,0:T(8,128)} custom-call(bf16[8,8,16,2048]{3,2,1,0:T(8,128)(2,1)} %bitcast.59), custom_call_target="tpu_custom_call" | custom-call | tf_op jit(solution)/shard_map/row_sum/pallas_call | solution.py:295
  63.5 1.4 multiply_reduce_fusion
  65.0 1.6 fusion.9
  66.8 1.2 convolution_convert_fusion.1
  68.0 63.6 %spread.1 = bf16[8,4,40,2176]{3,2,1,0:T(8,128)(2,1)} custom-call(bf16[4,40,2176]{2,1,0:T(8,128)(2,1)} %bitcast.65), custom_call_target="tpu_custom_call" | custom-call | tf_op jit(solution)/shard_map/spread/pallas_call | solution.py:186
  131.7 1.9 copy-done.1
  133.6 17.4 %experts.1 = bf16[1280,2048]{1,0:T(8,128)(2,1)} custom-call(bf16[1280,2176]{1,0:T(8,128)(2,1)} %bitcast.61, bf16[3,2048,256]{2,1,0:T(8,128)(2,1)S(1)} %copy-done.1, bf16[3,2048,256]{2,1,0:T(8,128)(2,1)} %up_ref.1, bf16[768,2048]{1,0:T(8,128)(2,1)} %bitcast.66), custom_call_target="tpu_custom_call" | custom-call | flops 12079595520 | bytes 20250624 | tf_op jit(solution)/shard_map/experts/pallas_call | solution.py:334
  150.9 54.0 %home_sum.1 = bf16[4,40,2048]{2,1,0:T(8,128)(2,1)} custom-call(bf16[8,4,40,2048]{3,2,1,0:T(8,128)(2,1)} %bitcast.62), custom_call_target="tpu_custom_call" | custom-call | tf_op jit(solution)/shard_map/home_sum/pallas_call | solution.py:295
  204.9 2.2 %fusion.1 = bf16[128,2048]{1,0:T(8,128)(2,1)} fusion(bf16[160,2048]{1,0:T(8,128)(2,1)} %bitcast.64, bf16[128,2048]{1,0:T(8,128)(2,1)S(1)} %get-tuple-element.6, s32[128]{0:T(128)S(1)} %multiply_add_fusion), kind=kOutput, calls=%fused_computation.7 | convolution fusion | flops 84692992 | bytes 1704448 | tf_op jit(solution)/shard_map/dot_general | solution.py:415
  (29 shorter events, 1.5 us)
Async XLA Ops:
  0.0 16.6 %copy-start = (bf16[256,2048]{1,0:T(8,128)(2,1)S(1)}, bf16[256,2048]{1,0:T(8,128)(2,1)}, u32[]{:S(2)}) copy-start(bf16[256,2048]{1,0:T(8,128)(2,1)} %param.18) | copy-start | bytes 3145732
  1.2 11.8 %collective-permute-start = (bf16[2,128,128]{2,1,0:T(8,128)(2,1)S(1)}, bf16[2,128,128]{2,1,0:T(8,128)(2,1)S(1)}, u32[]{:S(2)}, u32[]{:S(2)}) collective-permute-start(bf16[2,128,128]{2,1,0:T(8,128)(2,1)S(1)} %get-tuple-element.10), channel_id=1, source_target_pairs={{0,8},{8,16},{16,24},{1,9},{9,17},{17,25},{2,10},{10,18},{18,26},{... | collective-permute-start | bytes 196616 | tf_op jit(solution)/shard_map/ppermute | solution.py:27
  4.6 8.4 %collective-permute-start.1 = (bf16[2,128,128]{2,1,0:T(8,128)(2,1)S(1)}, bf16[2,128,128]{2,1,0:T(8,128)(2,1)S(1)}, u32[]{:S(2)}, u32[]{:S(2)}) collective-permute-start(bf16[2,128,128]{2,1,0:T(8,128)(2,1)S(1)} %get-tuple-element.11), channel_id=1, source_target_pairs={{8,0},{16,8},{24,16},{9,1},{17,9},{25,17},{10,2},{18,10},{26,18},{... | collective-permute-start | bytes 196616 | tf_op jit(solution)/shard_map/ppermute | solution.py:30
  13.6 0.7 copy-start.5
  19.8 45.1 %copy-start.2 = (bf16[128,2048]{1,0:T(8,128)(2,1)S(1)}, bf16[128,2048]{1,0:T(8,128)(2,1)}, u32[]{:S(2)}) copy-start(bf16[128,2048]{1,0:T(8,128)(2,1)} %param.19) | copy-start | bytes 1572868
  19.8 45.1 %copy-start.3 = (f32[2048]{0:T(1024)S(1)}, f32[2048]{0:T(1024)}, u32[]{:S(2)}) copy-start(f32[2048]{0:T(1024)} %param.20) | copy-start | bytes 24580
  19.9 46.7 %copy-start.4 = (f32[2048]{0:T(1024)S(1)}, f32[2048]{0:T(1024)}, u32[]{:S(2)}) copy-start(f32[2048]{0:T(1024)} %param.21) | copy-start | bytes 24580
  131.7 1.9 copy-start.1
